TPU v7x, 32 devices: a whole 2x2x4 slice. The times are simulated.
32 devices in a mesh: sp: 8 (over z, y), tp: 4 (over x, core).
Axes of the slice: x: 2, y: 2, z: 4, core: 2. Of those that a mesh axis runs over, the one named last changes fastest.
Arguments:
- queries: bfloat16 [2048, 2048], P('sp', 'tp'), may hold values from -9 to 9
- keys: bfloat16 [2048, 1024], P('sp', 'tp'), may hold values from -9 to 9
- values: bfloat16 [2048, 1024], P('sp', 'tp'), may hold values from -6 to 6
- lam: float32 [8], P('tp'), may hold values from 0.3 to 0.8
- diff_gain: float32 [256], replicated, may hold values from 0.1 to 1.9
- lin_query: bfloat16 [2048, 512], P('sp', 'tp'), may hold values from -6 to 6
- lin_key: bfloat16 [2048, 512], P('sp', 'tp'), may hold values from -6 to 6
- lin_value: bfloat16 [2048, 1024], P('sp', 'tp'), may hold values from -6 to 6
- decay_pre: float32 [2048, 512], P('sp', 'tp'), may hold values from -14 to 14
- lin_gain: float32 [1024], P('tp'), may hold values from 0.1 to 1.9
- w_out_diff: bfloat16 [2048, 4096], P('tp'), may hold values from -0.125 to 0.125
- w_out_lin: bfloat16 [1024, 4096], P('tp'), may hold values from -0.1875 to 0.1875
Outputs:
- mixed: bfloat16 [2048, 4096], P(('sp', 'tp'))
All inputs are finite; a program needn't handle non-finite values.
Results may differ from a plain program's by a relative error of at most 0.015.
Values may be sent and summed in bfloat16 or wider, within the bound.
A program may use at most 128 MiB of HBM per device.

v0:
```python
import math

import jax
import jax.numpy as jnp
from jax import lax
from jax.sharding import PartitionSpec as P

HEAD_DIM = 128
KEY_DIM = 128
VAL_DIM = 256
BLOCK = 64


norm_eps = 1e-06
gate_temp = 16.0
neg_large = -1e30
highest = lax.Precision.HIGHEST


def prefix(array, axis, combine, identity):
    size, mine = (lax.axis_size(axis), lax.axis_index(axis))
    everything = jax.tree.map(
        lambda part, kind: lax.all_gather(part.astype(kind), axis),
        array,
        (jnp.bfloat16, jnp.bfloat16),
    )
    start = jax.tree.map(
        lambda part, zero: jnp.broadcast_to(jnp.asarray(zero, part.dtype), part.shape),
        array,
        identity,
    )

    def hop(k, before):
        reached = k < mine
        new = combine(
            before, jax.tree.map(lambda part, own: part[k].astype(own.dtype), everything, array)
        )
        return jax.tree.map(lambda a, b: jnp.where(reached, a, b), new, before)

    return lax.fori_loop(0, size, hop, start)


def head_norm(mixed_in, gain):
    return (
        mixed_in
        * lax.rsqrt(jnp.mean(mixed_in * mixed_in, axis=-1, keepdims=True) + norm_eps)
        * gain
    )


def span_rows(row_count):
    if row_count <= 2048:
        return row_count
    return math.gcd(row_count, 2048)


def attend(carries, query_maps, key_maps, value_rows, query_pos):
    row_count = value_rows.shape[0]
    step_rows = span_rows(row_count)
    last_query = query_pos[-1]

    def visit(step_index, current):
        first_row = step_index * step_rows
        key_pos = first_row + jnp.arange(step_rows, dtype=jnp.int32)

        def compute(kept):
            value_part = lax.dynamic_slice_in_dim(value_rows, first_row, step_rows, 0)
            allowed = query_pos[:, None] >= key_pos[None, :]
            updated = []
            for query_map, key_map, running in zip(query_maps, key_maps, kept):
                old_top, old_total, old_numer = running
                key_part = lax.dynamic_slice_in_dim(key_map, first_row, step_rows, 0)
                scores = jnp.einsum(
                    "gjqd,sgd->gjqs", query_map, key_part, preferred_element_type=jnp.float32
                ) / math.sqrt(HEAD_DIM)
                scores = jnp.where(allowed, scores, neg_large)
                new_top = jnp.maximum(old_top, jnp.max(scores, axis=-1))
                weights = jnp.where(allowed, jnp.exp(scores - new_top[..., None]), 0.0)
                shrink = jnp.exp(old_top - new_top)
                new_total = old_total * shrink + jnp.sum(weights, axis=-1)
                new_numer = old_numer * shrink[..., None] + jnp.einsum(
                    "gjqs,sge->gjqe",
                    weights.astype(jnp.bfloat16),
                    value_part,
                    preferred_element_type=jnp.float32,
                )
                updated.append((new_top, new_total, new_numer))
            return tuple(updated)

        return lax.cond(first_row <= last_query, compute, lambda kept: kept, current)

    return lax.fori_loop(0, row_count // step_rows, visit, carries)


def decay_block(carry, inputs):
    run_state, passed = carry
    query_blk, key_blk, value_blk, decay_blk = inputs
    length = query_blk.shape[1]
    cumulative = jnp.cumsum(decay_blk, axis=1)
    lower_mask = jnp.tril(jnp.ones((length, length), dtype=bool))[None, :, :, None]
    spread = jnp.where(lower_mask, cumulative[:, :, None, :] - cumulative[:, None, :, :], 0.0)
    factor = jnp.where(lower_mask, jnp.exp(spread), 0.0)
    inner = jnp.einsum("htd,hsd,htsd->hts", query_blk, key_blk, factor, precision=highest)
    local_part = jnp.einsum("hts,hse->hte", inner, value_blk, precision=highest)
    carried = jnp.einsum(
        "htd,hde->hte", query_blk * jnp.exp(cumulative), run_state, precision=highest
    )
    last_sum = cumulative[:, -1:, :]
    new_state = jnp.exp(last_sum[:, 0, :])[..., None] * run_state + jnp.einsum(
        "hsd,hse->hde", key_blk * jnp.exp(last_sum - cumulative), value_blk, precision=highest
    )
    reach = query_blk * jnp.exp(passed[:, None, :] + cumulative)
    return ((new_state, passed + last_sum[:, 0, :]), (local_part + carried, reach))


def chain(earlier, later):
    return (earlier[0] + later[0], jnp.exp(later[0])[..., None] * earlier[1] + later[1])


def body(
    queries,
    keys,
    values,
    lam,
    diff_gain,
    lin_query,
    lin_key,
    lin_value,
    decay_pre,
    lin_gain,
    w_out_diff,
    w_out_lin,
):
    tok_rows = queries.shape[0]
    kv_here = keys.shape[1] // (2 * HEAD_DIM)
    heads_here = queries.shape[1] // (2 * HEAD_DIM)
    group_size = heads_here // kv_here
    query_pos = lax.axis_index("sp") * tok_rows + jnp.arange(tok_rows, dtype=jnp.int32)
    query_grid = queries.reshape(tok_rows, kv_here, group_size, 2, HEAD_DIM)
    query_maps = (
        query_grid[:, :, :, 0].transpose(1, 2, 0, 3),
        query_grid[:, :, :, 1].transpose(1, 2, 0, 3),
    )
    key_grid = keys.reshape(tok_rows, kv_here, 2, HEAD_DIM)
    value_grid = values.reshape(tok_rows, kv_here, VAL_DIM)
    blank = (
        jnp.full((kv_here, group_size, tok_rows), neg_large, jnp.float32),
        jnp.zeros((kv_here, group_size, tok_rows), jnp.float32),
        jnp.zeros((kv_here, group_size, tok_rows, VAL_DIM), jnp.float32),
    )
    pieces = (
        lax.all_gather(key_grid, "sp", axis=0, tiled=True),
        lax.all_gather(value_grid, "sp", axis=0, tiled=True),
    )
    first_acc, second_acc = attend(
        (blank, blank), query_maps, (pieces[0][:, :, 0], pieces[0][:, :, 1]), pieces[1], query_pos
    )
    lam_grid = lam.reshape(kv_here, group_size)
    attended = first_acc[2] / first_acc[1][..., None] - lam_grid[..., None, None] * (
        second_acc[2] / second_acc[1][..., None]
    )
    diff_out = head_norm(attended, diff_gain).astype(jnp.bfloat16)
    diff_out = diff_out.transpose(2, 0, 1, 3).reshape(tok_rows, heads_here * VAL_DIM)
    lin_heads_here = lin_query.shape[1] // KEY_DIM
    block_count = tok_rows // BLOCK

    def arrange(array, width):
        return (
            array.astype(jnp.float32)
            .reshape(block_count, BLOCK, lin_heads_here, width)
            .transpose(0, 2, 1, 3)
        )

    start_carry = (
        jnp.zeros((lin_heads_here, KEY_DIM, VAL_DIM), jnp.float32),
        jnp.zeros((lin_heads_here, KEY_DIM), jnp.float32),
    )
    (end_state, end_decay), (local_out, reach) = lax.scan(
        decay_block,
        start_carry,
        (
            arrange(lin_query, KEY_DIM) * KEY_DIM ** (-0.5),
            arrange(lin_key, KEY_DIM),
            arrange(lin_value, VAL_DIM),
            arrange(jax.nn.log_sigmoid(decay_pre) / gate_temp, KEY_DIM),
        ),
    )
    incoming = prefix(
        (end_decay, end_state), "sp", chain, (jnp.zeros_like(end_decay), jnp.zeros_like(end_state))
    )
    linear_rows = local_out + jnp.einsum("nhtd,hde->nhte", reach, incoming[1], precision=highest)
    linear_rows = linear_rows.transpose(0, 2, 1, 3).reshape(tok_rows, lin_heads_here, VAL_DIM)
    lin_out = head_norm(linear_rows, lin_gain.reshape(lin_heads_here, VAL_DIM)).astype(jnp.bfloat16)
    lin_out = lin_out.reshape(tok_rows, lin_heads_here * VAL_DIM)
    return lax.psum_scatter(
        (
            jnp.dot(diff_out, w_out_diff, preferred_element_type=jnp.float32)
            + jnp.dot(lin_out, w_out_lin, preferred_element_type=jnp.float32)
        ).astype(jnp.bfloat16),
        "tp",
        scatter_dimension=0,
        tiled=True,
    )


def solution(mesh):
    return jax.shard_map(
        body,
        mesh=mesh,
        in_specs=(
            P("sp", "tp"),
            P("sp", "tp"),
            P("sp", "tp"),
            P("tp"),
            P(),
            P("sp", "tp"),
            P("sp", "tp"),
            P("sp", "tp"),
            P("sp", "tp"),
            P("tp"),
            P("tp", None),
            P("tp", None),
        ),
        out_specs=P(("sp", "tp"), None),
        check_vma=False,
    )
```

profile of v0, /device:TPU:29, one launch (start us, length us, event | category | flops | bytes accessed | tf_op | source)
XLA Modules:
  0.0 154.3 jit_solution(5580665645317562080)
XLA Ops:
  6.5 1.8 %copy.36 = bf16[256,256]{0,1:T(8,128)(2,1)} copy(bf16[256,256]{1,0:T(8,128)(2,1)} %param.19) | data formatting | bytes 262144 | tf_op args[1]
  9.2 1.0 fusion.74
  11.1 0.9 convert.5
  12.0 0.9 convert_multiply_fusion
  12.9 24.5 %while.8 = (s32[]{:T(128)}, f32[1,128,256]{2,1,0:T(8,128)S(1)}, f32[1,128]{1,0:T(1,128)S(1)}, f32[4,1,64,256]{3,2,1,0:T(8,128)S(1)}, f32[4,1,64,128]{3,2,1,0:T(8...) while((s32[]{:T(128)}, f32[1,128,256]{2,1,0:T(8,128)S(1)}, ...), condition=%wide.region_9.10_spmd.clone, body=%wide.region_7.0_spmd.clone.sunk | while | flops 66765056 | bytes 5538459 | solution.py:178
  13.0 1.7 %exponential_select_fusion.4 = f32[64,64,128]{2,1,0:T(8,128)} fusion(f32[64,128]{1,0:T(8,128)S(1)} %bitcast.224, pred[64,64]{1,0:T(8,128)(4,1)S(1)} %iota_compare_fusion.2), kind=kLoop, calls=%fused_computation.46.clone.1 | loop fusion | flops 1572864 | bytes 2134016 | tf_op jit(solution)/shard_map/while/body/eval_jaxpr/jit(_where)/select_n | solution.py:102
  14.8 3.3 %fusion.107 = f32[64,64]{0,1:T(8,128)S(1)} fusion(f32[64,64,128]{2,1,0:T(8,128)} %exponential_select_fusion.4, f32[128,64]{0,1:T(8,128)S(1)} %get-tuple-element.553, f32[128,64]{0,1:T(8,128)S(1)} %dynamic-slice_bitcast_fusion.6), kind=kLoop, calls=%fused_computation.45.clone.1 | loop fusion | flops 1568768 | bytes 2179072 | tf_op jit(solution)/shard_map/while/body/eval_jaxpr/htd,hsd,htsd->hts/dot_general | solution.py:103
  19.1 1.7 %exponential_select_fusion.4 = f32[64,64,128]{2,1,0:T(8,128)} fusion(f32[64,128]{1,0:T(8,128)S(1)} %bitcast.224, pred[64,64]{1,0:T(8,128)(4,1)S(1)} %iota_compare_fusion.2), kind=kLoop, calls=%fused_computation.46.clone.1 | loop fusion | flops 1572864 | bytes 2134016 | tf_op jit(solution)/shard_map/while/body/eval_jaxpr/jit(_where)/select_n | solution.py:102
  20.9 3.3 %fusion.107 = f32[64,64]{0,1:T(8,128)S(1)} fusion(f32[64,64,128]{2,1,0:T(8,128)} %exponential_select_fusion.4, f32[128,64]{0,1:T(8,128)S(1)} %get-tuple-element.553, f32[128,64]{0,1:T(8,128)S(1)} %dynamic-slice_bitcast_fusion.6), kind=kLoop, calls=%fused_computation.45.clone.1 | loop fusion | flops 1568768 | bytes 2179072 | tf_op jit(solution)/shard_map/while/body/eval_jaxpr/htd,hsd,htsd->hts/dot_general | solution.py:103
  25.3 1.7 %exponential_select_fusion.4 = f32[64,64,128]{2,1,0:T(8,128)} fusion(f32[64,128]{1,0:T(8,128)S(1)} %bitcast.224, pred[64,64]{1,0:T(8,128)(4,1)S(1)} %iota_compare_fusion.2), kind=kLoop, calls=%fused_computation.46.clone.1 | loop fusion | flops 1572864 | bytes 2134016 | tf_op jit(solution)/shard_map/while/body/eval_jaxpr/jit(_where)/select_n | solution.py:102
  27.1 3.3 %fusion.107 = f32[64,64]{0,1:T(8,128)S(1)} fusion(f32[64,64,128]{2,1,0:T(8,128)} %exponential_select_fusion.4, f32[128,64]{0,1:T(8,128)S(1)} %get-tuple-element.553, f32[128,64]{0,1:T(8,128)S(1)} %dynamic-slice_bitcast_fusion.6), kind=kLoop, calls=%fused_computation.45.clone.1 | loop fusion | flops 1568768 | bytes 2179072 | tf_op jit(solution)/shard_map/while/body/eval_jaxpr/htd,hsd,htsd->hts/dot_general | solution.py:103
  31.4 1.7 %exponential_select_fusion.4 = f32[64,64,128]{2,1,0:T(8,128)} fusion(f32[64,128]{1,0:T(8,128)S(1)} %bitcast.224, pred[64,64]{1,0:T(8,128)(4,1)S(1)} %iota_compare_fusion.2), kind=kLoop, calls=%fused_computation.46.clone.1 | loop fusion | flops 1572864 | bytes 2134016 | tf_op jit(solution)/shard_map/while/body/eval_jaxpr/jit(_where)/select_n | solution.py:102
  33.2 3.3 %fusion.107 = f32[64,64]{0,1:T(8,128)S(1)} fusion(f32[64,64,128]{2,1,0:T(8,128)} %exponential_select_fusion.4, f32[128,64]{0,1:T(8,128)S(1)} %get-tuple-element.553, f32[128,64]{0,1:T(8,128)S(1)} %dynamic-slice_bitcast_fusion.6), kind=kLoop, calls=%fused_computation.45.clone.1 | loop fusion | flops 1568768 | bytes 2179072 | tf_op jit(solution)/shard_map/while/body/eval_jaxpr/htd,hsd,htsd->hts/dot_general | solution.py:103
  37.4 12.6 %all-gather.3 = bf16[8,1,128]{2,1,0:T(2,128)(2,1)S(1)} all-gather(bf16[1,1,128]{2,1,0:T(2,128)(2,1)S(1)} %convert_bitcast_fusion), channel_id=3, replica_groups=mesh['sp'=8,'tp'=4] {'sp'}, dimensions={0}, use_global_device_ids=true | all-gather | bytes 2304 | tf_op jit(solution)/shard_map/all_gather | solution.py:23
  50.0 26.8 %all-gather.2 = bf16[8,128,256]{2,1,0:T(8,128)(2,1)S(1)} all-gather(bf16[1,128,256]{2,1,0:T(8,128)(2,1)S(1)} %convert_element_type.81), channel_id=4, replica_groups=mesh['sp'=8,'tp'=4] {'sp'}, dimensions={0}, use_global_device_ids=true | all-gather | bytes 589824 | tf_op jit(solution)/shard_map/all_gather | solution.py:23
  76.8 1.1 while.9
  79.2 1.1 copy.35
  81.1 9.1 %all-gather.9.cloned.1.call-done = bf16[2048,256]{1,0:T(8,128)(2,1)} async-done(((bf16[256,256]{1,0:T(8,128)(2,1)}), bf16[2048,256]{1,0:T(8,128)(2,1)}) %all-gather.9.cloned.1.call-update) | async-done | bytes 1048592 | tf_op jit(solution)/shard_map/all_gather | solution.py:153
  90.2 13.8 %conditional.1 = (f32[1,2,256]{2,1,0:T(2,128)S(1)}, f32[1,2,256,256]{3,2,1,0:T(8,128)S(1)}, f32[1,2,256]{2,1,0:T(2,128)S(1)}, f32[1,2,256,256]{3,2,1,0:T(8,128)}) conditional(s32[]{:T(128)} %bitcast.15, (f32[1,2,256]{2,1,0:T(2,128)S(1)}, f32[1,2,256,256]{3,2,1,0:T(8,128)S(1)}) %tuple.46, (s32[256]{0:T(256)}, s32[2048]{0:T(1024)S(1)}, ...), branch_computations={%region_0.1_spmd, %region_1.6_spmd} | conditional | flops 1638928384 | bytes 48028760 | solution.py:90
  90.2 1.0 broadcast_compare_fusion
  91.2 2.3 %copy.38 = bf16[2048,1,2,128]{3,0,2,1:T(8,128)(2,1)} copy(bf16[2048,1,2,128]{0,3,2,1:T(8,128)(2,1)} %get-tuple-element.405) | data formatting | bytes 2097152 | tf_op jit(solution)/shard_map
  93.5 1.9 %fusion.27 = f32[2,256,2048]{2,1,0:T(8,128)S(1)} fusion(bf16[2048,1,2,128]{3,0,2,1:T(8,128)(2,1)} %copy.38, bf16[1,2,256,128]{2,3,1,0:T(8,128)(2,1)S(1)} %get-tuple-element.404), kind=kOutput, calls=%fused_computation.24 | convolution fusion | flops 268435456 | bytes 4849664 | tf_op jit(solution)/shard_map/while/body/eval_jaxpr/cond/branch_1_fun/gjqd,sgd->gjqs/dot_general | solution.py:73
  95.4 2.0 %fusion.1 = (f32[2,256]{1,0:T(2,128)S(1)}, f32[2,256]{1,0:T(2,128)S(1)}, f32[2,256,2048]{2,1,0:T(8,128)S(1)}) fusion(pred[256,2048]{1,0:T(8,128)(4,1)S(1)} %broadcast_compare_fusion, f32[2,256,2048]{2,1,0:T(8,128)S(1)} %fusion.27, bf16[2048,1,2,128]{3,0,2,1:T(8,128)(2,1)S(1)} %copy-done.1, bf16[1,2,256,128]{2,3,1,0:T(8,128)(2,1)S(1)} %get-tuple-element.409), kind=kOutput, calls=%fused_computation.5 | convolution fusion | flops 274725888 | bytes 9572352 | tf_op jit(solution)/shard_map/while/body/eval_jaxpr/cond/branch_1_fun/gjqd,sgd->gjqs/dot_general | solution.py:73
  97.4 2.5 %fusion.5 = (f32[2,256]{1,0:T(2,128)S(1)}, f32[2,256]{1,0:T(2,128)S(1)}) fusion(f32[2,256,2048]{2,1,0:T(8,128)S(1)} %get-tuple-element.455, f32[2,256]{1,0:T(2,128)S(1)} %get-tuple-element.450, pred[256,2048]{1,0:T(8,128)(4,1)S(1)} %broadcast_compare_fusion, f32[2,256]{1,0:T(2,128)S(1)} %get-tuple-element.456, f32[2,256,2048]{2,1,0:T(8,128)S(1)} %fusion.27), kind=kLoop, calls=%fused_computation.9 | loop fusion | flops 10484736 | bytes 8921088 | tf_op jit(solution)/shard_map/while/body/eval_jaxpr/cond/branch_1_fun/reduce_sum | solution.py:80
  100.0 2.2 %fusion.18 = f32[1,2,256,256]{3,2,1,0:T(8,128)} fusion(f32[2,256,2048]{2,1,0:T(8,128)S(1)} %get-tuple-element.455, f32[2,256]{1,0:T(2,128)S(1)} %get-tuple-element.450, pred[256,2048]{1,0:T(8,128)(4,1)S(1)} %broadcast_compare_fusion, bf16[2048,1,256]{2,0,1:T(8,128)(2,1)S(1)} %copy-done.4, f32[1,2,256,256]{3,2,1,0:T(8,128)S(1)} %get-tuple-element.296, ...), kind=kOutput, calls=%fused_computation.16 | convolution fusion | flops 542375936 | bytes 6819840 | tf_op jit(solution)/shard_map/while/body/eval_jaxpr/cond/branch_1_fun/gjqs,sge->gjqe/dot_general | solution.py:81
  102.2 1.7 %fusion.21 = f32[1,2,256,256]{3,2,1,0:T(8,128)S(1)} fusion(f32[2,256,2048]{2,1,0:T(8,128)S(1)} %fusion.27, f32[2,256]{1,0:T(2,128)S(1)} %get-tuple-element.456, pred[256,2048]{1,0:T(8,128)(4,1)S(1)} %broadcast_compare_fusion, bf16[2048,1,256]{2,0,1:T(8,128)(2,1)S(1)} %copy-done.4, f32[1,2,256,256]{3,2,1,0:T(8,128)S(1)} %get-tuple-element.296, ...), kind=kOutput, calls=%fused_computation.17 | convolution fusion | flops 542375936 | bytes 6819840 | tf_op jit(solution)/shard_map/while/body/eval_jaxpr/cond/branch_1_fun/gjqs,sge->gjqe/dot_general | solution.py:81
  104.1 1.2 copy.41
  105.3 1.0 copy.40
  106.3 1.2 multiply_reduce_fusion
  108.3 3.5 %fusion.77 = f32[256,4096]{1,0:T(8,128)S(1)} fusion(bf16[256,512]{0,1:T(8,128)(2,1)S(1)} %bitcast.225, bf16[512,4096]{1,0:T(8,128)(2,1)} %param.28), kind=kOutput, calls=%fused_computation.111 | convolution fusion | flops 1073741824 | bytes 8650752 | tf_op jit(solution)/shard_map/dot_general | solution.py:197
  111.8 2.1 %fusion.69 = bf16[256,4096]{1,0:T(8,128)(2,1)} fusion(f32[256,4096]{1,0:T(8,128)S(1)} %fusion.77, bf16[256,256]{1,0:T(8,128)(2,1)S(1)} %fusion.72, bf16[256,4096]{1,0:T(8,128)(2,1)S(1)} %copy-done), kind=kOutput, calls=%fused_computation.89 | convolution fusion | flops 538968064 | bytes 8519680 | tf_op jit(solution)/shard_map/dot_general | solution.py:198
  114.0 33.8 %reduce-scatter.2.cloned.1.call-done = bf16[64,4096]{1,0:T(8,128)(2,1)} async-done(((bf16[256,4096]{1,0:T(8,128)(2,1)}), bf16[64,4096]{1,0:T(8,128)(2,1)}) %reduce-scatter.2.cloned.1.call-update) | async-done | bytes 524304 | tf_op jit(solution)/shard_map/reduce_scatter | solution.py:195
  (99 shorter events, 8.8 us)
Async XLA Ops:
  6.5 105.3 %copy-start = (bf16[256,4096]{1,0:T(8,128)(2,1)S(1)}, bf16[256,4096]{1,0:T(8,128)(2,1)}, u32[]{:S(2)}) copy-start(bf16[256,4096]{1,0:T(8,128)(2,1)} %param.29) | copy-start | bytes 6291460
  6.5 74.5 %all-gather.7.cloned.1.call-start = ((), (), s32[]{:S(2)}) async-start(), calls=%async_computation.1 | async-start | bytes 1179648 | tf_op jit(solution)/shard_map/all_gather | solution.py:152
  8.4 81.8 %all-gather.9.cloned.1.call-start = ((), (), s32[]{:S(2)}) async-start(), calls=%async_computation.3 | async-start | bytes 1179648 | tf_op jit(solution)/shard_map/all_gather | solution.py:153
  9.1 138.7 %reduce-scatter.2.cloned.1.call-start = ((), (), s32[]{:S(2)}) async-start(), calls=%async_computation.2 | async-start | bytes 2621440 | tf_op jit(solution)/shard_map/reduce_scatter | solution.py:195
  37.4 43.5 %copy-start.2 = (f32[256]{0:T(256)S(1)}, f32[256]{0:T(256)}, u32[]{:S(2)}) copy-start(f32[256]{0:T(256)} %param.27) | copy-start | bytes 3076
  77.9 2.8 %copy-start.3 = (s32[256]{0:T(256)}, s32[256]{0:T(256)S(1)}, u32[]{:S(2)}) copy-start(s32[256]{0:T(256)S(1)} %iota_add_fusion) | copy-start | bytes 3076
  93.5 1.9 %copy-start.1 = (bf16[2048,1,2,128]{3,0,2,1:T(8,128)(2,1)S(1)}, bf16[2048,1,2,128]{3,0,2,1:T(8,128)(2,1)}, u32[]{:S(2)}) copy-start(bf16[2048,1,2,128]{3,0,2,1:T(8,128)(2,1)} %copy.38) | copy-start | bytes 3145732 | tf_op jit(solution)/shard_map/while/body/eval_jaxpr/cond
  97.4 2.6 %copy-start.4 = (bf16[2048,1,256]{2,0,1:T(8,128)(2,1)S(1)}, bf16[2048,1,256]{2,0,1:T(8,128)(2,1)}, u32[]{:S(2)}) copy-start(bf16[2048,1,256]{2,0,1:T(8,128)(2,1)} %get-tuple-element.297) | copy-start | bytes 3145732 | tf_op jit(solution)/shard_map/while/body/eval_jaxpr/cond
Sparse Core Ops, SparseCore 0:
  9.4 36.8 all-gather.6
  48.4 41.7 all-gather.8
  114.1 33.6 reduce-scatter.1
where the time goes:
time: 157 us; the launch traced here: 154 us
  waiting for transfers between devices  43.7 us (28%)
  blocking collectives  39.3 us (25%)
  other arithmetic  30.9 us (20%)
  matrix products  17.3 us (11%)
  between operations  14 us (9%)
  local copies, waits for them, and re-layouts  8.33 us (5%)
    all_gather x2, blocking collectives, prefix(): lax.all_gather(part.astype(kind), axis)  39.3 us
    reduce_scatter x1, waiting for transfers between devices, body(): lax.psum_scatter((jnp.dot(diff_out, w_out_diff, preferred_element_type=jn...  33.8 us
    dot_general x4, other arithmetic, decay_block(): jnp.einsum('htd,hsd,htsd->hts', query_blk, key_blk, factor, precision=hig...  13.2 us
    all_gather x1, waiting for transfers between devices, body(): lax.all_gather(value_grid, 'sp', axis=0, tiled=True)  9.13 us
    select_n x4, other arithmetic, decay_block(): factor = jnp.where(lower_mask, jnp.exp(spread), 0.0)  6.99 us
    dot_general x2, matrix products, compute(): jnp.einsum('gjqs,sge->gjqe', weights.astype(jnp.bfloat16), value_part, pr...  3.92 us
    dot_general x2, matrix products, compute(): jnp.einsum('gjqd,sgd->gjqs', query_map, key_part, preferred_element_type=...  3.84 us
    dot_general x1, matrix products, body(): jnp.dot(diff_out, w_out_diff, preferred_element_type=jnp.float32)  3.51 us
  transfers between devices with their start and end apart: 3, of which 2 were waited for; matrix products, arithmetic and copies ran while one was open for 20% of the time, Pallas kernels for 0%

commit v1 on v0

v1 whole, which is shorter than its diff:
```python
import functools
import math

import jax
import jax.numpy as jnp
from jax import lax
from jax.experimental import pallas as pl
from jax.experimental.pallas import tpu as pltpu
from jax.sharding import PartitionSpec as P

HEAD_DIM = 128
KEY_DIM = 128
VAL_DIM = 256
BLOCK = 64
PIECE = 512

norm_eps = 1e-06
gate_temp = 16.0
neg_large = -1e30
highest = lax.Precision.HIGHEST
MESH = pl.DeviceIdType.MESH
F32 = jnp.float32
BF16 = jnp.bfloat16


def dot(a, b, dims, precision=None):
    return lax.dot_general(
        a, b, (dims, ((), ())), precision=precision, preferred_element_type=F32
    )


NN = ((1,), (0,))
NT = ((1,), (1,))
TN = ((0,), (0,))


def head_norm(rows, gain):
    return rows * lax.rsqrt(jnp.mean(rows * rows, axis=-1, keepdims=True) + norm_eps) * gain


def kernel(
    n_sp,
    n_tp,
    q_ref,
    k_ref,
    v_ref,
    lam_ref,
    dgain_ref,
    lq_ref,
    lk_ref,
    lv_ref,
    pre_ref,
    lgain_ref,
    wd_ref,
    wl_ref,
    out_ref,
    zk,
    zv,
    yk,
    yv,
    qs,
    top,
    total,
    numer,
    msg,
    got,
    chain_in,
    chain_out,
    own_state,
    reach,
    rows_ref,
    act,
    weights,
    part,
    pair_buf,
    sum_buf,
    own_sum,
    cross_buf,
    w_sem,
    zk_send,
    zk_recv,
    zv_send,
    zv_recv,
    yk_send,
    yk_recv,
    yv_send,
    yv_recv,
    s_send,
    s_recv,
    c_send,
    c_recv,
    p_send,
    p_recv,
    x_send,
    x_recv,
):
    outer_n = n_sp // 2
    half = n_tp // 2
    tok = q_ref.shape[0]
    kv_here = k_ref.shape[1] // (2 * HEAD_DIM)
    heads = q_ref.shape[1] // (2 * HEAD_DIM)
    group = heads // kv_here
    lin_heads = lq_ref.shape[1] // KEY_DIM
    diff_rows = wd_ref.shape[0]
    me = lax.axis_index("sp")
    tp = lax.axis_index("tp")
    outer = me // 2
    inner = lax.rem(me, 2)
    mate = outer * 2 + (1 - inner)
    ahead = me + 2
    behind = me - 2
    tp_x = tp // 2
    tp_c = lax.rem(tp, 2)
    tp_mate = tp_x * 2 + (1 - tp_c)
    has_next = outer < outer_n - 1
    has_prev = outer > 0

    w_copies = (
        pltpu.make_async_copy(wd_ref, weights.at[pl.ds(0, diff_rows)], w_sem.at[0]),
        pltpu.make_async_copy(
            wl_ref, weights.at[pl.ds(diff_rows, wl_ref.shape[0])], w_sem.at[1]
        ),
    )
    for copy in w_copies:
        copy.start()

    barrier = pltpu.get_barrier_semaphore()

    def greet(where):
        pl.semaphore_signal(barrier, inc=1, device_id=where, device_id_type=MESH)

    greet({"sp": mate})
    greet({"tp": tp_mate})
    for step in range(1, half):
        greet({"tp": lax.rem(tp_x + step, half) * 2 + tp_c})

    @pl.when(has_next)
    def _():
        greet({"sp": ahead})

    @pl.when(has_prev)
    def _():
        greet({"sp": behind})

    pl.semaphore_wait(
        barrier, 1 + half + has_next.astype(jnp.int32) + has_prev.astype(jnp.int32)
    )

    def remote(src, dst, send, recv, where):
        return pltpu.make_async_remote_copy(
            src_ref=src,
            dst_ref=dst,
            send_sem=send,
            recv_sem=recv,
            device_id=where,
            device_id_type=MESH,
        )

    def z_k(s, src):
        return remote(src, zk.at[s + 1], zk_send.at[s], zk_recv.at[s + 1], {"sp": ahead})

    def z_v(s, src):
        return remote(src, zv.at[s + 1], zv_send.at[s], zv_recv.at[s + 1], {"sp": ahead})

    def y_k(s, src):
        return remote(src, yk.at[s], yk_send.at[s], yk_recv.at[s], {"sp": mate})

    def y_v(s, src):
        return remote(src, yv.at[s], yv_send.at[s], yv_recv.at[s], {"sp": mate})

    @pl.when(has_next)
    def _():
        z_k(0, k_ref).start()

    @pl.when(inner == 0)
    def _():
        y_k(0, k_ref).start()

    @pl.when(has_next)
    def _():
        z_v(0, v_ref).start()

    length = math.gcd(tok, BLOCK)
    low = lax.broadcasted_iota(jnp.int32, (length, length), 0) >= lax.broadcasted_iota(
        jnp.int32, (length, length), 1
    )
    tri = low.astype(F32)
    for h in range(lin_heads):
        kc = pl.ds(h * KEY_DIM, KEY_DIM)
        vc = pl.ds(h * VAL_DIM, VAL_DIM)
        state = None
        passed = jnp.zeros((1, KEY_DIM), F32)
        for b in range(tok // length):
            r = pl.ds(b * length, length)
            pre = pre_ref[r, kc]
            log_decay = (jnp.minimum(pre, 0.0) - jnp.log1p(jnp.exp(-jnp.abs(pre)))) / gate_temp
            cumulative = dot(tri, log_decay, NN, highest)
            last = cumulative[length - 1 :, :]
            query = lq_ref[r, kc].astype(F32) * (KEY_DIM**-0.5) * jnp.exp(cumulative)
            key = lk_ref[r, kc].astype(F32)
            value = lv_ref[r, vc].astype(F32)
            inside = dot(query, key * jnp.exp(-cumulative), NT, highest)
            inside = jnp.where(low, inside, 0.0)
            rows = dot(inside, value, NN, highest)
            fresh = dot(value, key * jnp.exp(last - cumulative), TN, highest)
            if state is not None:
                rows = rows + dot(query, state, NT, highest)
                fresh = fresh + jnp.exp(last) * state
            rows_ref[r, vc] = rows
            reach[r, kc] = query * jnp.exp(passed)
            state = fresh
            passed = passed + last
        own_state[h, pl.ds(0, VAL_DIM), :] = state
        own_state[h, pl.ds(VAL_DIM, 8), :] = jnp.broadcast_to(passed, (8, KEY_DIM))
        msg[h, pl.ds(0, VAL_DIM), :] = state.astype(BF16)
        high = passed.astype(BF16).astype(F32)
        pick = lax.broadcasted_iota(jnp.int32, (16, KEY_DIM), 0) < 8
        msg[h, pl.ds(VAL_DIM, 16), :] = jnp.where(pick, high, passed - high).astype(BF16)

    s_copy = remote(msg, got, s_send, s_recv, {"sp": mate})
    s_copy.start()

    @pl.when(inner == 0)
    def _():
        y_v(0, v_ref).start()

    for g in range(kv_here):
        for m in range(2):
            for j in range(group):
                col = ((g * group + j) * 2 + m) * HEAD_DIM
                qs[g, m, pl.ds(j * tok, tok), :] = q_ref[:, pl.ds(col, HEAD_DIM)]

    rate = math.log2(math.e) / math.sqrt(HEAD_DIM)
    stacked = group * tok

    def attend(key_ref, value_ref, first):
        for g in range(kv_here):
            value = value_ref[:, pl.ds(g * VAL_DIM, VAL_DIM)]
            for m in range(2):
                key = key_ref[:, pl.ds((g * 2 + m) * HEAD_DIM, HEAD_DIM)]
                scores = dot(qs[g, m], key, NT)
                if first:
                    at_row = lax.rem(lax.broadcasted_iota(jnp.int32, (stacked, tok), 0), tok)
                    at_col = lax.broadcasted_iota(jnp.int32, (stacked, tok), 1)
                    scores = jnp.where(at_row >= at_col, scores, neg_large)
                best = jnp.max(scores, axis=-1, keepdims=True)
                if not first:
                    old = top[g, m]
                    best = jnp.maximum(old, best)
                expo = jnp.exp2((scores - best) * rate)
                add = jnp.sum(expo, axis=-1, keepdims=True)
                grown = dot(expo.astype(BF16), value, NN)
                if first:
                    total[g, m] = add
                    numer[g, m] = grown
                else:
                    shrink = jnp.exp2((old - best) * rate)
                    total[g, m] = total[g, m] * shrink + add
                    numer[g, m] = numer[g, m] * shrink + grown
                top[g, m] = best

    attend(k_ref, v_ref, True)

    def from_mate(t):
        y_k(t, yk.at[t]).wait_recv()
        y_v(t, yv.at[t]).wait_recv()
        attend(yk.at[t], yv.at[t], False)

    def hop(s, carry):
        remote(zk.at[s], zk.at[s], zk_send.at[s], zk_recv.at[s], {"sp": mate}).wait_recv()

        @pl.when(has_next)
        def _():
            z_k(s, zk.at[s]).start()

        y_k(s, zk.at[s]).start()
        remote(zv.at[s], zv.at[s], zv_send.at[s], zv_recv.at[s], {"sp": mate}).wait_recv()

        @pl.when(has_next)
        def _():
            z_v(s, zv.at[s]).start()

        y_v(s, zv.at[s]).start()
        attend(zk.at[s], zv.at[s], False)

        @pl.when((s > 1) | (inner == 1))
        def _():
            from_mate(s - 1)

        return carry

    lax.fori_loop(1, outer + 1, hop, 0)

    s_copy.wait_recv()
    c_copy = remote(chain_out, chain_in, c_send, c_recv, {"sp": ahead})

    @pl.when(has_prev)
    def _():
        c_copy.wait_recv()

    @pl.when(jnp.logical_not(has_prev))
    def _():
        chain_in[...] = jnp.zeros_like(chain_in)

    for h in range(lin_heads):
        mine = own_state[h, pl.ds(0, VAL_DIM), :]
        mine_decay = own_state[h, pl.ds(VAL_DIM, 8), :][:1]
        theirs = got[h, pl.ds(0, VAL_DIM), :].astype(F32)
        tail = got[h, pl.ds(VAL_DIM, 16), :].astype(F32)
        theirs_decay = tail[:1] + tail[8:9]
        before = chain_in[h].astype(F32)
        to_first = jnp.exp(theirs_decay) * before + theirs
        incoming = jnp.where(inner == 1, to_first, before)
        both = jnp.exp(mine_decay) * to_first + mine
        other = jnp.exp(theirs_decay) * (jnp.exp(mine_decay) * before + mine) + theirs
        chain_out[h] = jnp.where(inner == 1, both, other).astype(BF16)
        own_state[h, pl.ds(0, VAL_DIM), :] = incoming

    @pl.when(has_next)
    def _():
        c_copy.start()

    for h in range(lin_heads):
        kc = pl.ds(h * KEY_DIM, KEY_DIM)
        vc = pl.ds(h * VAL_DIM, VAL_DIM)
        rows = rows_ref[:, vc] + dot(
            reach[:, kc], own_state[h, pl.ds(0, VAL_DIM), :], NT, highest
        )
        act[:, pl.ds(diff_rows + h * VAL_DIM, VAL_DIM)] = head_norm(
            rows, lgain_ref[:, vc]
        ).astype(BF16)

    @pl.when(has_prev | (inner == 1))
    def _():
        from_mate(outer)

    for g in range(kv_here):
        for j in range(group):
            h = g * group + j
            r = pl.ds(j * tok, tok)
            attended = numer[g, 0, r, :] / total[g, 0, r, :] - lam_ref[h] * (
                numer[g, 1, r, :] / total[g, 1, r, :]
            )
            act[:, pl.ds(h * VAL_DIM, VAL_DIM)] = head_norm(attended, dgain_ref[...]).astype(BF16)

    for copy in w_copies:
        copy.wait()

    width = part.shape[-1]
    pieces = part.shape[0]
    rows_each = tok // n_tp

    def pair_copy(j):
        return remote(
            part.at[j, 1 - tp_c], pair_buf.at[j], p_send.at[j], p_recv.at[j], {"tp": tp_mate}
        )

    def cross_copy(j, step):
        to = lax.rem(tp_x + step, half)
        return remote(
            sum_buf.at[j, step - 1],
            cross_buf.at[j, step - 1],
            x_send.at[j, step - 1],
            x_recv.at[j, step - 1],
            {"tp": to * 2 + tp_c},
        )

    def reduce_pair(j):
        pair_copy(j).wait_recv()
        for step in range(1, half):
            to = lax.rem(tp_x + step, half)
            sum_buf[j, step - 1] = (
                part[j, tp_c, to].astype(F32) + pair_buf[j, to].astype(F32)
            ).astype(BF16)
            cross_copy(j, step).start()
        own_sum[j] = part[j, tp_c, tp_x].astype(F32) + pair_buf[j, tp_x].astype(F32)

    def project(j, carry):
        cols = pl.ds(pl.multiple_of(j * width, width), width)
        piece = dot(act[...], weights[:, cols], NN).astype(BF16)
        for a in range(half):
            for c in range(2):
                part[j, c, a] = piece[(a * 2 + c) * rows_each : (a * 2 + c + 1) * rows_each]
        pair_copy(j).start()

        @pl.when(j > 0)
        def _():
            reduce_pair(j - 1)

        return carry

    lax.fori_loop(0, pieces, project, 0)
    reduce_pair(pieces - 1)

    def finish(j, carry):
        cols = pl.ds(pl.multiple_of(j * width, width), width)
        whole = own_sum[j]
        for step in range(1, half):
            cross_copy(j, step).wait_recv()
            whole = whole + cross_buf[j, step - 1].astype(F32)
        out_ref[:, cols] = whole.astype(BF16)
        pair_copy(j).wait_send()
        for step in range(1, half):
            cross_copy(j, step).wait_send()
        return carry

    lax.fori_loop(0, pieces, finish, 0)

    s_copy.wait_send()

    @pl.when(inner == 0)
    def _():
        y_k(0, k_ref).wait_send()
        y_v(0, v_ref).wait_send()

    @pl.when(has_next)
    def _():
        z_k(0, k_ref).wait_send()
        z_v(0, v_ref).wait_send()
        c_copy.wait_send()

    def drain(s, carry):
        y_k(s, zk.at[s]).wait_send()
        y_v(s, zv.at[s]).wait_send()

        @pl.when(has_next)
        def _():
            z_k(s, zk.at[s]).wait_send()
            z_v(s, zv.at[s]).wait_send()

        return carry

    lax.fori_loop(1, outer + 1, drain, 0)


def body(
    n_sp,
    n_tp,
    queries,
    keys,
    values,
    lam,
    diff_gain,
    lin_query,
    lin_key,
    lin_value,
    decay_pre,
    lin_gain,
    w_out_diff,
    w_out_lin,
):
    tok = queries.shape[0]
    kv_here = keys.shape[1] // (2 * HEAD_DIM)
    heads = queries.shape[1] // (2 * HEAD_DIM)
    lin_heads = lin_query.shape[1] // KEY_DIM
    model = w_out_diff.shape[1]
    in_rows = w_out_diff.shape[0] + w_out_lin.shape[0]
    stacked = heads // kv_here * tok
    width = math.gcd(model, PIECE)
    pieces = model // width
    half = n_tp // 2
    outer_n = n_sp // 2
    rows_each = tok // n_tp
    vmem = pl.BlockSpec(memory_space=pltpu.VMEM)
    anywhere = pl.BlockSpec(memory_space=pl.ANY)
    smem = pl.BlockSpec(memory_space=pltpu.SMEM)
    dma = pltpu.SemaphoreType.DMA
    return pl.pallas_call(
        functools.partial(kernel, n_sp, n_tp),
        out_shape=jax.ShapeDtypeStruct((rows_each, model), BF16),
        in_specs=[vmem] * 3 + [smem] + [vmem] * 6 + [anywhere] * 2,
        out_specs=vmem,
        scratch_shapes=[
            pltpu.VMEM((outer_n, *keys.shape), BF16),
            pltpu.VMEM((outer_n, *values.shape), BF16),
            pltpu.VMEM((outer_n, *keys.shape), BF16),
            pltpu.VMEM((outer_n, *values.shape), BF16),
            pltpu.VMEM((kv_here, 2, stacked, HEAD_DIM), BF16),
            pltpu.VMEM((kv_here, 2, stacked, 1), F32),
            pltpu.VMEM((kv_here, 2, stacked, 1), F32),
            pltpu.VMEM((kv_here, 2, stacked, VAL_DIM), F32),
            pltpu.VMEM((lin_heads, VAL_DIM + 16, KEY_DIM), BF16),
            pltpu.VMEM((lin_heads, VAL_DIM + 16, KEY_DIM), BF16),
            pltpu.VMEM((lin_heads, VAL_DIM, KEY_DIM), BF16),
            pltpu.VMEM((lin_heads, VAL_DIM, KEY_DIM), BF16),
            pltpu.VMEM((lin_heads, VAL_DIM + 8, KEY_DIM), F32),
            pltpu.VMEM(lin_query.shape, F32),
            pltpu.VMEM(lin_value.shape, F32),
            pltpu.VMEM((tok, in_rows), BF16),
            pltpu.VMEM((in_rows, model), BF16),
            pltpu.VMEM((pieces, 2, half, rows_each, width), BF16),
            pltpu.VMEM((pieces, half, rows_each, width), BF16),
            pltpu.VMEM((pieces, half - 1, rows_each, width), BF16),
            pltpu.VMEM((pieces, rows_each, width), F32),
            pltpu.VMEM((pieces, half - 1, rows_each, width), BF16),
            dma((2,)),
        ]
        + [dma((outer_n,))] * 8
        + [dma] * 4
        + [dma((pieces,))] * 2
        + [dma((pieces, half - 1))] * 2,
        compiler_params=pltpu.CompilerParams(
            collective_id=0, has_side_effects=True, vmem_limit_bytes=60 * 1024 * 1024
        ),
    )(
        queries,
        keys,
        values,
        lam,
        diff_gain.reshape(1, -1),
        lin_query,
        lin_key,
        lin_value,
        decay_pre,
        lin_gain.reshape(1, -1),
        w_out_diff,
        w_out_lin,
    )


def solution(mesh):
    return jax.shard_map(
        functools.partial(body, mesh.shape["sp"], mesh.shape["tp"]),
        mesh=mesh,
        in_specs=(
            P("sp", "tp"),
            P("sp", "tp"),
            P("sp", "tp"),
            P("tp"),
            P(),
            P("sp", "tp"),
            P("sp", "tp"),
            P("sp", "tp"),
            P("sp", "tp"),
            P("tp"),
            P("tp", None),
            P("tp", None),
        ),
        out_specs=P(("sp", "tp"), None),
        check_vma=False,
    )
```

time: 157 us -> 48.9 us (0.31); the launches traced: 154 us -> 48.7 us
  Pallas kernels: 0 us -> 46.9 us
  waiting for transfers between devices: 43.7 us -> 0 us
  blocking collectives: 39.3 us -> 0 us
  other arithmetic: 30.9 us -> 0 us
  matrix products: 17.3 us -> 0 us
  between operations: 14 us -> 0.01 us
  local copies, waits for them, and re-layouts: 8.33 us -> 1.87 us
    pallas_call x0 -> x1, Pallas kernels: none -> 46.9 us  [body(): pl.pallas_call(functools.partial(kernel, n_sp, n_tp), out_shape=jax.Shape...]
    all_gather x2 -> x0, blocking collectives: 39.3 us -> none  [prefix(): lax.all_gather(part.astype(kind), axis)]
    reduce_scatter x1 -> x0, waiting for transfers between devices: 33.8 us -> none  [body(): lax.psum_scatter((jnp.dot(diff_out, w_out_diff, preferred_element_type=jn...]
    dot_general x19 -> x0, matrix products: 17.3 us -> none  [the longest x2 3.92 us: compute(): jnp.einsum('gjqs,sge->gjqe', weights.astype(jnp.bfloat16), value_part, pr...]
    dot_general x4 -> x0, other arithmetic: 13.2 us -> none  [decay_block(): jnp.einsum('htd,hsd,htsd->hts', query_blk, key_blk, factor, precision=hig...]
    all_gather x2 -> x0, waiting for transfers between devices: 9.15 us -> none  [the longest x1 9.13 us: body(): lax.all_gather(value_grid, 'sp', axis=0, tiled=True)]
    select_n x12 -> x0, other arithmetic: 7.74 us -> none  [the longest x4 6.99 us: decay_block(): factor = jnp.where(lower_mask, jnp.exp(spread), 0.0)]
    reduce_sum x2 -> x0, other arithmetic: 3.76 us -> none  [the longest x1 2.54 us: compute(): new_total = old_total * shrink + jnp.sum(weights, axis=-1)]
  transfers between devices with their start and end apart: 3 -> 0, of which waited for: 2 -> 0; matrix products, arithmetic and copies ran while one was open for 20% -> 0% of each run, Pallas kernels for 0% -> 0%
where the time goes in v1:
time: 48.9 us; the launch traced here: 48.7 us
  Pallas kernels  46.9 us (96%)
  local copies, waits for them, and re-layouts  1.87 us (4%)
    pallas_call x1, Pallas kernels, body(): pl.pallas_call(functools.partial(kernel, n_sp, n_tp), out_shape=jax.Shape...  46.9 us
    unnamed x1, local copies, waits for them, and re-layouts  1.87 us

profile of v1, /device:TPU:29, one launch (start us, length us, event | category | flops | bytes accessed | tf_op | source)
XLA Modules:
  0.0 48.7 jit_solution(14708583225078852453)
XLA Ops:
  0.0 46.9 %shard_map.118 = bf16[64,4096]{1,0:T(8,128)(2,1)} custom-call(bf16[256,512]{1,0:T(8,128)(2,1)} %q_ref.1, bf16[256,256]{1,0:T(8,128)(2,1)} %k_ref.1, bf16[256,256]{1,0:T(8,128)(2,1)} %v_ref.1, f32[2]{0:T(128)} %lam_ref.1, f32[1,256]{1,0:T(1,128)} %bitcast.2, bf16[256,128]{1,0:T(8,128)(2,1)} %lq_ref.1, bf16[256,128]{1,0:T(8,128)(2,1)} %lk_ref.1, ...), custom_call_target="tpu_custom_call" | custom-call | tf_op jit(solution)/shard_map/pallas_call | solution.py:468
  46.9 1.9 %copy.14 = bf16[64,4096]{1,0:T(8,128)(2,1)} copy(bf16[64,4096]{1,0:T(8,128)(2,1)} %shard_map.118) | data formatting | bytes 1048576

commit v2 on v1

--- a/solution.py
+++ b/solution.py
@@ -180,6 +180,72 @@
     def _():
         z_v(0, v_ref).start()
 
+    @pl.when(inner == 0)
+    def _():
+        y_v(0, v_ref).start()
+
+    for g in range(kv_here):
+        for m in range(2):
+            for j in range(group):
+                col = ((g * group + j) * 2 + m) * HEAD_DIM
+                qs[g, m, pl.ds(j * tok, tok), :] = q_ref[:, pl.ds(col, HEAD_DIM)]
+
+    rate = math.log2(math.e) / math.sqrt(HEAD_DIM)
+    stacked = group * tok
+
+    def attend(key_ref, value_ref, first, ready=None):
+        kept = {}
+        for g in range(kv_here):
+            for m in range(2):
+                key = key_ref[:, pl.ds((g * 2 + m) * HEAD_DIM, HEAD_DIM)]
+                scores = dot(qs[g, m], key, NT)
+                if first:
+                    at_row = lax.rem(lax.broadcasted_iota(jnp.int32, (stacked, tok), 0), tok)
+                    at_col = lax.broadcasted_iota(jnp.int32, (stacked, tok), 1)
+                    scores = jnp.where(at_row >= at_col, scores, neg_large)
+                best = jnp.max(scores, axis=-1, keepdims=True)
+                if not first:
+                    old = top[g, m]
+                    best = jnp.maximum(old, best)
+                expo = jnp.exp2((scores - best) * rate)
+                add = jnp.sum(expo, axis=-1, keepdims=True)
+                top[g, m] = best
+                shrink = None
+                if first:
+                    total[g, m] = add
+                else:
+                    shrink = jnp.exp2((old - best) * rate)
+                    total[g, m] = total[g, m] * shrink + add
+                kept[g, m] = (expo.astype(BF16), shrink)
+        if ready is not None:
+            ready()
+        for g in range(kv_here):
+            value = value_ref[:, pl.ds(g * VAL_DIM, VAL_DIM)]
+            for m in range(2):
+                expo, shrink = kept[g, m]
+                grown = dot(expo, value, NN)
+                numer[g, m] = grown if first else numer[g, m] * shrink + grown
+
+    attend(k_ref, v_ref, True)
+
+    def pass_key(s):
+        remote(zk.at[s], zk.at[s], zk_send.at[s], zk_recv.at[s], {"sp": mate}).wait_recv()
+
+        @pl.when(has_next)
+        def _():
+            z_k(s, zk.at[s]).start()
+
+        y_k(s, zk.at[s]).start()
+
+    def pass_value(s):
+        remote(zv.at[s], zv.at[s], zv_send.at[s], zv_recv.at[s], {"sp": mate}).wait_recv()
+
+        @pl.when(has_next)
+        def _():
+            z_v(s, zv.at[s]).start()
+
+        y_v(s, zv.at[s]).start()
+
     length = math.gcd(tok, BLOCK)
     low = lax.broadcasted_iota(jnp.int32, (length, length), 0) >= lax.broadcasted_iota(
         jnp.int32, (length, length), 1
@@ -210,6 +276,12 @@
             reach[r, kc] = query * jnp.exp(passed)
             state = fresh
             passed = passed + last
+            if h == lin_heads - 1 and b == (tok // length) // 2 - 1:
+
+                @pl.when(has_prev)
+                def _():
+                    pass_key(1)
+
         own_state[h, pl.ds(0, VAL_DIM), :] = state
         own_state[h, pl.ds(VAL_DIM, 8), :] = jnp.broadcast_to(passed, (8, KEY_DIM))
         msg[h, pl.ds(0, VAL_DIM), :] = state.astype(BF16)
@@ -220,67 +292,21 @@
     s_copy = remote(msg, got, s_send, s_recv, {"sp": mate})
     s_copy.start()
 
-    @pl.when(inner == 0)
-    def _():
-        y_v(0, v_ref).start()
-
-    for g in range(kv_here):
-        for m in range(2):
-            for j in range(group):
-                col = ((g * group + j) * 2 + m) * HEAD_DIM
-                qs[g, m, pl.ds(j * tok, tok), :] = q_ref[:, pl.ds(col, HEAD_DIM)]
-
-    rate = math.log2(math.e) / math.sqrt(HEAD_DIM)
-    stacked = group * tok
-
-    def attend(key_ref, value_ref, first):
-        for g in range(kv_here):
-            value = value_ref[:, pl.ds(g * VAL_DIM, VAL_DIM)]
-            for m in range(2):
-                key = key_ref[:, pl.ds((g * 2 + m) * HEAD_DIM, HEAD_DIM)]
-                scores = dot(qs[g, m], key, NT)
-                if first:
-                    at_row = lax.rem(lax.broadcasted_iota(jnp.int32, (stacked, tok), 0), tok)
-                    at_col = lax.broadcasted_iota(jnp.int32, (stacked, tok), 1)
-                    scores = jnp.where(at_row >= at_col, scores, neg_large)
-                best = jnp.max(scores, axis=-1, keepdims=True)
-                if not first:
-                    old = top[g, m]
-                    best = jnp.maximum(old, best)
-                expo = jnp.exp2((scores - best) * rate)
-                add = jnp.sum(expo, axis=-1, keepdims=True)
-                grown = dot(expo.astype(BF16), value, NN)
-                if first:
-                    total[g, m] = add
-                    numer[g, m] = grown
-                else:
-                    shrink = jnp.exp2((old - best) * rate)
-                    total[g, m] = total[g, m] * shrink + add
-                    numer[g, m] = numer[g, m] * shrink + grown
-                top[g, m] = best
-
-    attend(k_ref, v_ref, True)
+    @pl.when(has_prev)
+    def _():
+        pass_value(1)
+
 
     def from_mate(t):
         y_k(t, yk.at[t]).wait_recv()
-        y_v(t, yv.at[t]).wait_recv()
-        attend(yk.at[t], yv.at[t], False)
+        attend(yk.at[t], yv.at[t], False, lambda: y_v(t, yv.at[t]).wait_recv())
 
     def hop(s, carry):
-        remote(zk.at[s], zk.at[s], zk_send.at[s], zk_recv.at[s], {"sp": mate}).wait_recv()
-
-        @pl.when(has_next)
+        @pl.when(s > 1)
         def _():
-            z_k(s, zk.at[s]).start()
-
-        y_k(s, zk.at[s]).start()
-        remote(zv.at[s], zv.at[s], zv_send.at[s], zv_recv.at[s], {"sp": mate}).wait_recv()
-
-        @pl.when(has_next)
-        def _():
-            z_v(s, zv.at[s]).start()
-
-        y_v(s, zv.at[s]).start()
+            pass_key(s)
+            pass_value(s)
+
         attend(zk.at[s], zv.at[s], False)
 
         @pl.when((s > 1) | (inner == 1))

time: 48.9 us -> 47 us (0.961)
  Pallas kernels: 46.9 us -> 45 us
    pallas_call x1, Pallas kernels: 46.9 us -> 45 us  [body(): pl.pallas_call(functools.partial(kernel, n_sp, n_tp), out_shape=jax.Shape...]
where the time goes in v2:
time: 47 us; the launch traced here: 46.8 us
  Pallas kernels  45 us (96%)
  local copies, waits for them, and re-layouts  1.87 us (4%)
    pallas_call x1, Pallas kernels, body(): pl.pallas_call(functools.partial(kernel, n_sp, n_tp), out_shape=jax.Shape...  45 us
    unnamed x1, local copies, waits for them, and re-layouts  1.87 us

profile of v2, /device:TPU:29, one launch (start us, length us, event | category | flops | bytes accessed | tf_op | source)
XLA Modules:
  0.0 46.8 jit_solution(8697870001559112583)
XLA Ops:
  0.0 45.0 %shard_map.118 = bf16[64,4096]{1,0:T(8,128)(2,1)} custom-call(bf16[256,512]{1,0:T(8,128)(2,1)} %q_ref.1, bf16[256,256]{1,0:T(8,128)(2,1)} %k_ref.1, bf16[256,256]{1,0:T(8,128)(2,1)} %v_ref.1, f32[2]{0:T(128)} %lam_ref.1, f32[1,256]{1,0:T(1,128)} %bitcast.2, bf16[256,128]{1,0:T(8,128)(2,1)} %lq_ref.1, bf16[256,128]{1,0:T(8,128)(2,1)} %lk_ref.1, ...), custom_call_target="tpu_custom_call" | custom-call | tf_op jit(solution)/shard_map/pallas_call | solution.py:494
  45.0 1.9 %copy.14 = bf16[64,4096]{1,0:T(8,128)(2,1)} copy(bf16[64,4096]{1,0:T(8,128)(2,1)} %shard_map.118) | data formatting | bytes 1048576

commit v3 on v2

--- a/solution.py
+++ b/solution.py
@@ -12,7 +12,8 @@
 KEY_DIM = 128
 VAL_DIM = 256
 BLOCK = 64
-PIECE = 512
+PIECE = 256
+LAG = 3
 
 norm_eps = 1e-06
 gate_temp = 16.0
@@ -409,14 +410,19 @@
                 part[j, c, a] = piece[(a * 2 + c) * rows_each : (a * 2 + c + 1) * rows_each]
         pair_copy(j).start()
 
-        @pl.when(j > 0)
+        @pl.when(j >= LAG)
         def _():
-            reduce_pair(j - 1)
+            reduce_pair(j - LAG)
 
         return carry
 
     lax.fori_loop(0, pieces, project, 0)
-    reduce_pair(pieces - 1)
+
+    def reduce_rest(j, carry):
+        reduce_pair(j)
+        return carry
+
+    lax.fori_loop(max(pieces - LAG, 0), pieces, reduce_rest, 0)
 
     def finish(j, carry):
         cols = pl.ds(pl.multiple_of(j * width, width), width)

time: 47 us -> 47.4 us (level)
  no operation moved by 1% of the time
where the time goes in v3:
time: 47.4 us; the launch traced here: 47.2 us
  Pallas kernels  45.3 us (96%)
  local copies, waits for them, and re-layouts  1.87 us (4%)
    pallas_call x1, Pallas kernels, body(): pl.pallas_call(functools.partial(kernel, n_sp, n_tp), out_shape=jax.Shape...  45.3 us
    unnamed x1, local copies, waits for them, and re-layouts  1.87 us

profile of v3, /device:TPU:29, one launch (start us, length us, event | category | flops | bytes accessed | tf_op | source)
XLA Modules:
  0.0 47.2 jit_solution(5515418360894984369)
XLA Ops:
  0.0 45.3 %shard_map.118 = bf16[64,4096]{1,0:T(8,128)(2,1)} custom-call(bf16[256,512]{1,0:T(8,128)(2,1)} %q_ref.1, bf16[256,256]{1,0:T(8,128)(2,1)} %k_ref.1, bf16[256,256]{1,0:T(8,128)(2,1)} %v_ref.1, f32[2]{0:T(128)} %lam_ref.1, f32[1,256]{1,0:T(1,128)} %bitcast.2, bf16[256,128]{1,0:T(8,128)(2,1)} %lq_ref.1, bf16[256,128]{1,0:T(8,128)(2,1)} %lk_ref.1, ...), custom_call_target="tpu_custom_call" | custom-call | tf_op jit(solution)/shard_map/pallas_call | solution.py:500
  45.3 1.9 %copy.14 = bf16[64,4096]{1,0:T(8,128)(2,1)} copy(bf16[64,4096]{1,0:T(8,128)(2,1)} %shard_map.118) | data formatting | bytes 1048576
